TPU v7x, 32 devices: a whole 2x2x4 slice. The times are simulated.
32 devices in a mesh: ep: 8 (over z, core), tp: 4 (over y, x).
Axes of the slice: x: 2, y: 2, z: 4, core: 2. Of those that a mesh axis runs over, the one named last changes fastest.
Arguments:
- mixer_value_input: bfloat16 [2048, 4096], P('ep', 'tp'), may hold values from -6 to 6
- input_state_matrix: bfloat16 [2048, 2048], P('ep', 'tp'), may hold values from -6 to 6
- output_state_matrix: bfloat16 [2048, 2048], P('ep', 'tp'), may hold values from -6 to 6
- output_gate_input: bfloat16 [2048, 4096], P('ep', 'tp'), may hold values from -6 to 6
- step_input: float32 [2048, 64], P('ep', 'tp'), may hold values from -6 to -2
- extra_log_decay: float32 [2048, 64], P('ep', 'tp'), may hold values from -1 to 0
- head_log_decay: float32 [64], P('tp'), may hold values from -10 to 1
- head_skip_scale: float32 [64], P('tp'), may hold values from 0.5 to 2
- value_kernel: float32 [4, 4096], P(None, 'tp'), may hold values from -3 to 3
- input_matrix_kernel: float32 [4, 2048], P(None, 'tp'), may hold values from -3 to 3
- output_matrix_kernel: float32 [4, 2048], P(None, 'tp'), may hold values from -3 to 3
- mixer_norm_scale: float32 [4096], P('tp'), may hold values from 0.1 to 1.9
- mixer_output_weight: bfloat16 [4096, 2048], P(None, 'tp'), may hold values from -0.09375 to 0.09375
- second_token_rows: bfloat16 [2048, 2048], P('ep'), may hold values from -6 to 6
- expert_norm_scale: float32 [2048], replicated, may hold values from 0.1 to 1.9
- routed_expert_index: int32 [2048, 4], P('ep'), may hold values from 0 to 15, all different within a row; in each aligned block of 256 rows (0 to 255, 256 to 511, ...) at most 96 rows name the same one
- routed_expert_weight: float32 [2048, 4], P('ep'), may hold values from 0.1 to 1
- routed_gate_weight: bfloat16 [16, 2048, 1024], P('ep', None, 'tp'), may hold values from -0.125 to 0.125
- routed_up_weight: bfloat16 [16, 2048, 1024], P('ep', None, 'tp'), may hold values from -0.125 to 0.125
- routed_down_weight: bfloat16 [16, 1024, 2048], P('ep', None, 'tp'), may hold values from -0.1875 to 0.1875
- shared_gate_weight: bfloat16 [2048, 1024], P(None, 'tp'), may hold values from -0.125 to 0.125
- shared_up_weight: bfloat16 [2048, 1024], P(None, 'tp'), may hold values from -0.125 to 0.125
- shared_down_weight: bfloat16 [1024, 2048], P(None, 'tp'), may hold values from -0.1875 to 0.1875
Outputs:
- mixer_output: bfloat16 [2048, 2048], P('ep', 'tp')
- routed_out: bfloat16 [2048, 2048], P('ep', 'tp')
Inputs may be any that keep to these rules, and one draw needn't show every extreme that they name: `routed_expert_index`: in each aligned block of 256 rows (the rows of one index of ep) no expert is named more than 96 times, a bound that some block reaches.
All inputs are finite; a program needn't handle non-finite values.
Results may differ from a plain program's by a relative error of at most 0.012.
Values may be sent and summed in bfloat16 or wider, within the bound.
A program may use at most 64 MiB of HBM per device.

v0:
```python
import jax
import jax.numpy as jnp
from jax import lax
from jax.sharding import PartitionSpec as P

HEAD_DIM = 64
STATE = 128
CONV_TAPS = 4
BLOCK = 128
TOP_K = 4
epsilon = 1e-05
precise = lax.Precision.HIGHEST


def passed_along(x, axis, by):
    size = lax.axis_size(axis)
    pairs = [(i, i + by) for i in range(size) if 0 <= i + by < size]
    return lax.ppermute(x, axis, pairs)


def carried_in(total_log, state, axis):
    size = lax.axis_size(axis)
    place = lax.axis_index(axis)
    log = passed_along(total_log, axis, 1)
    hold = passed_along(state.astype(jnp.bfloat16), axis, 1).astype(jnp.float32)
    by = 1
    while by < size - 1:
        before = passed_along(hold.astype(jnp.bfloat16), axis, by).astype(jnp.float32)
        hold = hold + jnp.exp(log)[:, None, None] * before
        log = log + passed_along(log, axis, by)
        by *= 2
    return hold


def conv_silu(tail_rows, source, weights):
    length = source.shape[0]
    padded = jnp.concatenate([tail_rows, source], axis=0)
    total_sum = jnp.zeros(source.shape, jnp.float32)
    for tap_index in range(CONV_TAPS):
        total_sum = (
            total_sum
            + padded[tap_index : tap_index + length].astype(jnp.float32) * weights[tap_index]
        )
    return jax.nn.silu(total_sum).astype(jnp.bfloat16)


def carry_blocks(carried, inputs):
    block_decay, block_state = inputs
    return (carried * block_decay[:, None, None] + block_state, carried)


def earlier_counts(mask, rows):
    at = jnp.arange(rows)
    tri = (at[:, None] < at[None, :]).astype(jnp.bfloat16)
    return lax.dot_general(
        mask.astype(jnp.bfloat16),
        tri,
        (((mask.ndim - 1,), (0,)), ((), ())),
        preferred_element_type=jnp.float32,
    )


def on_device(
    mixer_value_input,
    input_state_matrix,
    output_state_matrix,
    output_gate_input,
    step_input,
    extra_log_decay,
    head_log_decay,
    head_skip_scale,
    value_kernel,
    input_matrix_kernel,
    output_matrix_kernel,
    mixer_norm_scale,
    mixer_output_weight,
    second_token_rows,
    expert_norm_scale,
    routed_expert_index,
    routed_expert_weight,
    routed_gate_weight,
    routed_up_weight,
    routed_down_weight,
    shared_gate_weight,
    shared_up_weight,
    shared_down_weight,
):
    length = mixer_value_input.shape[0]
    heads_local = step_input.shape[1]
    width_x = mixer_value_input.shape[1]
    width_b = input_state_matrix.shape[1]
    groups_local = width_b // STATE
    head_ratio = heads_local // groups_local
    nblocks = length // BLOCK
    lead_row = length - CONV_TAPS + 1
    edge_rows = jnp.concatenate(
        [
            mixer_value_input[lead_row:],
            input_state_matrix[lead_row:],
            output_state_matrix[lead_row:],
        ],
        axis=1,
    )
    tail_rows = passed_along(edge_rows, "ep", 1)
    rows_local = second_token_rows.shape[0]
    model_width = second_token_rows.shape[1]
    local_experts = routed_gate_weight.shape[0]
    ep_count = lax.axis_size("ep")
    experts = local_experts * ep_count
    capacity = max(2, 3 * rows_local * TOP_K // (2 * experts))
    col_width = model_width // lax.axis_size("tp")
    rows_wide = second_token_rows.astype(jnp.float32)
    normed = (
        rows_wide
        * lax.rsqrt(jnp.mean(rows_wide * rows_wide, axis=-1, keepdims=True) + epsilon)
        * expert_norm_scale
    ).astype(jnp.bfloat16)
    ids = routed_expert_index.T.astype(jnp.float32)
    id_rows = -(-ids.size // col_width)
    id_block = jnp.pad(
        ids.astype(jnp.bfloat16).reshape(-1), (0, id_rows * col_width - ids.size)
    ).reshape(id_rows, col_width)
    id_block = jnp.pad(id_block, ((0, -id_rows % 8), (0, 0)))
    my_columns = lax.dynamic_slice_in_dim(normed, lax.axis_index("tp") * col_width, col_width, 1)
    outgoing, value_rows, in_rows, out_rows = lax.optimization_barrier(
        (
            jnp.concatenate([my_columns, id_block], axis=0),
            mixer_value_input,
            input_state_matrix,
            output_state_matrix,
        )
    )
    everyone = lax.all_gather(outgoing, "ep", axis=0)
    values = conv_silu(tail_rows[:, :width_x], value_rows, value_kernel)
    in_mat = conv_silu(tail_rows[:, width_x : width_x + width_b], in_rows, input_matrix_kernel)
    out_mat = conv_silu(tail_rows[:, width_x + width_b :], out_rows, output_matrix_kernel)
    step_length = jax.nn.softplus(step_input)
    decay_logarithm = -jnp.exp(head_log_decay)[None, :] * step_length + extra_log_decay
    running = jnp.cumsum(decay_logarithm.reshape(nblocks, BLOCK, heads_local), axis=1)
    value_wide = values.astype(jnp.float32).reshape(nblocks, BLOCK, heads_local, HEAD_DIM)
    scaled = value_wide * step_length.reshape(nblocks, BLOCK, heads_local)[..., None]
    in_blocks = in_mat.reshape(nblocks, BLOCK, groups_local, STATE)
    out_blocks = out_mat.reshape(nblocks, BLOCK, groups_local, STATE)
    scores = jnp.einsum(
        "bign,bjgn->bgij", out_blocks, in_blocks, preferred_element_type=jnp.float32
    )
    scores = jnp.repeat(scores, head_ratio, axis=1)
    spread = jnp.transpose(running[:, :, None, :] - running[:, None, :, :], (0, 3, 1, 2))
    lower_mask = jnp.tril(jnp.ones((BLOCK, BLOCK), bool))[None, None]
    decay_mat = jnp.where(lower_mask, jnp.exp(jnp.where(lower_mask, spread, 0.0)), 0.0)
    inside = jnp.einsum("bhij,bjhp->bihp", scores * decay_mat, scaled, precision=precise)
    out_head = jnp.repeat(out_blocks.astype(jnp.float32), head_ratio, axis=2)
    in_head = jnp.repeat(in_blocks.astype(jnp.float32), head_ratio, axis=2)
    block_logs = running[:, -1]
    to_end = jnp.exp(block_logs[:, None, :] - running)
    block_state = jnp.einsum("bjhn,bjh,bjhp->bhpn", in_head, to_end, scaled, precision=precise)
    start_state = jnp.zeros((heads_local, HEAD_DIM, STATE), jnp.float32)
    local_total, local_prev = lax.scan(
        carry_blocks, start_state, (jnp.exp(block_logs), block_state)
    )
    before_logs = jnp.cumsum(block_logs, axis=0) - block_logs
    everyone, local_total = lax.optimization_barrier((everyone, local_total))
    incoming = carried_in(jnp.sum(block_logs, axis=0), local_total, "ep")
    their_rows = everyone[:, :rows_local]
    their_ids = everyone[:, rows_local : rows_local + id_rows].reshape(ep_count, -1)
    their_ids = their_ids[:, : ids.size].reshape(ep_count, TOP_K, rows_local).astype(jnp.float32)
    mine = (lax.axis_index("ep") * local_experts + jnp.arange(local_experts)).astype(jnp.float32)
    named = jnp.any(their_ids[:, None] == mine[None, :, None, None], axis=2)
    seat = jnp.where(named, earlier_counts(named, rows_local), -1.0)
    seats = jnp.arange(capacity, dtype=jnp.float32)
    pick = (seat[:, :, None, :] == seats[None, None, :, None]).astype(jnp.bfloat16)
    arrived = jnp.stack(
        [
            jnp.einsum("bsr,brd->bsd", pick[:, j], their_rows, preferred_element_type=jnp.float32)
            .astype(jnp.bfloat16)
            .reshape(ep_count * capacity, col_width)
            for j in range(local_experts)
        ]
    )
    column_piece = lax.all_gather(arrived, "tp", axis=2, tiled=True)
    column_piece, incoming = lax.optimization_barrier((column_piece, incoming))
    entering = local_prev + jnp.exp(before_logs)[:, :, None, None] * incoming[None]
    carried_term = (
        jnp.einsum("bihn,bhpn->bihp", out_head, entering, precision=precise)
        * jnp.exp(running)[..., None]
    )
    mixed_heads = (inside + carried_term).reshape(length, heads_local, HEAD_DIM)
    mixed_heads = mixed_heads + head_skip_scale[None, :, None] * value_wide.reshape(
        length, heads_local, HEAD_DIM
    )
    gated_heads = mixed_heads * jax.nn.silu(output_gate_input.astype(jnp.float32)).reshape(
        length, heads_local, HEAD_DIM
    )
    grouped = gated_heads.reshape(length, groups_local, head_ratio * HEAD_DIM)
    grouped = grouped * lax.rsqrt(jnp.mean(grouped * grouped, axis=-1, keepdims=True) + epsilon)
    mixer_normed = (grouped.reshape(length, width_x) * mixer_norm_scale).astype(jnp.bfloat16)
    gate_pre = jnp.einsum(
        "esd,edf->esf", column_piece, routed_gate_weight, preferred_element_type=jnp.float32
    )
    up_pre = jnp.einsum(
        "esd,edf->esf", column_piece, routed_up_weight, preferred_element_type=jnp.float32
    )
    hidden = (jax.nn.silu(gate_pre) * up_pre).astype(jnp.bfloat16)
    shared_hidden = (
        jax.nn.silu(jnp.dot(normed, shared_gate_weight, preferred_element_type=jnp.float32))
        * jnp.dot(normed, shared_up_weight, preferred_element_type=jnp.float32)
    ).astype(jnp.bfloat16)
    whole_hidden = lax.all_gather(hidden, "tp", axis=2, tiled=True)
    both = lax.all_gather(
        jnp.concatenate([mixer_normed, shared_hidden], axis=1), "tp", axis=1, tiled=True
    ).reshape(length, lax.axis_size("tp"), -1)
    whole_mix = both[:, :, :width_x].reshape(length, -1)
    whole_shared = both[:, :, width_x:].reshape(length, -1)
    mixer_output = jnp.dot(
        whole_mix, mixer_output_weight, preferred_element_type=jnp.float32
    ).astype(jnp.bfloat16)
    expert_result = jnp.einsum(
        "esf,efd->esd", whole_hidden, routed_down_weight, preferred_element_type=jnp.float32
    ).astype(jnp.bfloat16)
    going = jnp.concatenate(
        [expert_result[j].reshape(ep_count, capacity, col_width) for j in range(local_experts)],
        axis=1,
    )
    returned = lax.all_to_all(going, "ep", split_axis=0, concat_axis=0, tiled=True)
    returned = returned.reshape(experts * capacity, col_width)
    kinds = jnp.arange(experts, dtype=jnp.float32)
    chosen = ids[:, None, :] == kinds[None, :, None]
    count = earlier_counts(jnp.any(chosen, axis=0), rows_local)
    position = jnp.sum(jnp.where(chosen, count[None], 0.0), axis=1)
    slot = (ids * capacity + position).T.astype(jnp.int32)
    columns = jnp.arange(experts * capacity, dtype=jnp.int32)[None, :]
    spread = jnp.zeros((rows_local, experts * capacity), jnp.float32)
    for k in range(TOP_K):
        spread = spread + jnp.where(
            slot[:, k : k + 1] == columns, routed_expert_weight[:, k : k + 1], 0.0
        )
    high = lax.reduce_precision(spread, 8, 7)
    low = (spread - high).astype(jnp.bfloat16)
    routed_sum = jnp.dot(
        high.astype(jnp.bfloat16), returned, preferred_element_type=jnp.float32
    ) + jnp.dot(low, returned, preferred_element_type=jnp.float32)
    shared_result = jnp.dot(whole_shared, shared_down_weight, preferred_element_type=jnp.float32)
    routed_out = (routed_sum + shared_result).astype(jnp.bfloat16)
    return (mixer_output, routed_out)


def solution(mesh):
    return jax.shard_map(
        on_device,
        mesh=mesh,
        in_specs=(
            P("ep", "tp"),
            P("ep", "tp"),
            P("ep", "tp"),
            P("ep", "tp"),
            P("ep", "tp"),
            P("ep", "tp"),
            P("tp"),
            P("tp"),
            P(None, "tp"),
            P(None, "tp"),
            P(None, "tp"),
            P("tp"),
            P(None, "tp"),
            P("ep", None),
            P(),
            P("ep", None),
            P("ep", None),
            P("ep", None, "tp"),
            P("ep", None, "tp"),
            P("ep", None, "tp"),
            P(None, "tp"),
            P(None, "tp"),
            P(None, "tp"),
        ),
        out_specs=(P("ep", "tp"), P("ep", "tp")),
        check_vma=False,
    )
```

profile of v0, /device:TPU:0, one launch (start us, length us, event | category | flops | bytes accessed | tf_op | source)
XLA Modules:
  0.0 239.8 jit_solution(12581473368572431942)
XLA Ops:
  9.6 1.1 copy.77
  10.7 3.2 %collective-permute-start = (bf16[3,2048]{0,1:T(8,128)(2,1)}, bf16[3,2048]{0,1:T(8,128)(2,1)}, u32[]{:S(2)}, u32[]{:S(2)}) collective-permute-start(bf16[3,2048]{0,1:T(8,128)(2,1)} %copy.77), channel_id=1, source_target_pairs={{0,4},{4,8},{8,12},{12,16},{16,20},{20,24},{24,28},{1,5},{5,9},{9,... | collective-permute-start | bytes 36872 | tf_op jit(solution)/shard_map/ppermute | solution.py:18
  13.9 1.5 fusion.1
  16.4 1.1 copy-done.3
  23.6 1.3 copy.78
  26.7 3.4 %multiply_convert_fusion.2 = (bf16[256,512]{1,0:T(8,128)(2,1)}, bf16[256,512]{1,0:T(8,128)(2,1)}) fusion(bf16[256,512]{1,0:T(8,128)(2,1)} %param.26, bf16[3,512]{1,0:T(4,128)(2,1)} %copy.81, f32[512]{0:T(512)} %bitcast.141, f32[512]{0:T(512)} %bitcast.142, f32[512]{0:T(512)} %bitcast.140, f32[512]{0:T(512)} %bitcast.139, f32[512]{0:T(512)} %bitcast.145, ...), kind=kLoop, calls=%fused_computation.103 | loop fusion | flops 6553600 | bytes 1071104 | tf_op jit(solution)/shard_map/convert_element_type | solution.py:44
  32.9 2.9 %fusion.71 = f32[256,1024]{0,1:T(8,128)} fusion(f32[1024]{0:T(1024)} %bitcast.134, bf16[256,1024]{0,1:T(8,128)(2,1)S(1)} %copy.78, f32[1024]{0:T(1024)} %bitcast.135, bf16[3,1024]{0,1:T(8,128)(2,1)S(1)} %slice.176, f32[1024]{0:T(1024)} %bitcast.133, f32[1024]{0:T(1024)} %bitcast.132), kind=kLoop, calls=%fused_computation.106 | loop fusion | flops 6815744 | bytes 1595392 | tf_op jit(solution)/shard_map/convert_element_type | solution.py:140
  35.8 2.7 %reshape.132 = f32[2,128,16,64]{1,0,3,2:T(2,128)} reshape(f32[256,1024]{0,1:T(8,128)} %fusion.71) | data formatting | bytes 2097152 | tf_op jit(solution)/shard_map/reshape | solution.py:140
  38.6 3.0 %broadcast_multiply_fusion = (f32[2,128,16,64]{1,0,3,2:T(2,128)S(1)}, f32[2,128,16,64]{1,0,3,2:T(2,128)}) fusion(f32[2,128,16]{1,0,2:T(2,128)S(1)} %copy.88, f32[2,128,16,64]{1,0,3,2:T(2,128)} %reshape.132, f32[2,128,16]{1,0,2:T(2,128)} %mul.326), kind=kLoop, calls=%fused_computation.102 | loop fusion | flops 524288 | bytes 3178496 | tf_op jit(solution)/shard_map/bjhn,bjh,bjhp->bhpn/dot_general | solution.py:156
  41.8 3.1 %fusion.37 = f32[2,16,64,128]{3,2,1,0:T(8,128)} fusion(f32[2,128,16,128]{3,1,2,0:T(8,128)S(1)} %bitcast.120, f32[2,128,16,64]{1,0,3,2:T(2,128)S(1)} %get-tuple-element.78), kind=kOutput, calls=%fused_computation.55 | convolution fusion | flops 402653184 | bytes 4194304 | tf_op jit(solution)/shard_map/bjhn,bjh,bjhp->bhpn/dot_general | solution.py:156
  44.9 4.0 %while.13 = (s32[]{:T(128)}, f32[16,64,128]{2,1,0:T(8,128)S(1)}, f32[2,16,64,128]{3,2,1,0:T(8,128)}, f32[2,16]{1,0:T(2,128)S(1)}, f32[2,16,64,128]{3,2,1,0:T(8,128)}, /*index=5*/s32[]{:T(128)}, s32[]{:T(128)}) while((s32[]{:T(128)}, f32[16,64,128]{2,1,0:T(8,128)S(1)}, f32[2,16,64,128]{3,2,1,0:T(8,128)}, f32[2,16]{1,0:T(2,128)S(1)}, ...), condition=%wide.region_3.4_spmd.clone, body=%wide.region_2.3_spmd.clone.sunk | while | flops 524291 | bytes 2621740 | solution.py:158
  45.8 1.2 bitcast_add_fusion.4
  47.8 1.2 bitcast_add_fusion.4
  51.3 2.3 fusion.18
  54.0 1.3 pad_maximum_fusion
  55.5 3.0 %collective-permute-start.1 = (bf16[16,64,128]{2,1,0:T(8,128)(2,1)S(1)}, bf16[16,64,128]{2,1,0:T(8,128)(2,1)S(1)}, u32[]{:S(2)}, u32[]{:S(2)}) collective-permute-start(bf16[16,64,128]{2,1,0:T(8,128)(2,1)S(1)} %convert_element_type.179), channel_id=1, source_target_pairs={{0,4},{4,8},{8,12},{12,16},{16,20},{20,24},{24,28},{1,5},{5,9},{9,... | collective-permute-start | bytes 786440 | tf_op jit(solution)/shard_map/ppermute | solution.py:18
  58.5 1.1 collective-permute-done.1
  59.7 4.5 %collective-permute-start.3 = (bf16[16,64,128]{2,1,0:T(8,128)(2,1)S(1)}, bf16[16,64,128]{2,1,0:T(8,128)(2,1)S(1)}, u32[]{:S(2)}, u32[]{:S(2)}) collective-permute-start(bf16[16,64,128]{2,1,0:T(8,128)(2,1)S(1)} %collective-permute-done.1), channel_id=1, source_target_pairs={{0,4},{4,8},{8,12},{12,16},{16,20},{20,24},{24,28},{1,5},{5,9},{9,... | collective-permute-start | bytes 786440 | tf_op jit(solution)/shard_map/ppermute | solution.py:18
  64.2 4.4 %collective-permute-start.2 = (f32[16]{0:T(128)S(1)}, f32[16]{0:T(128)S(1)}, u32[]{:S(2)}, u32[]{:S(2)}) collective-permute-start(f32[16]{0:T(128)S(1)} %copy-done.31), channel_id=1, source_target_pairs={{0,4},{4,8},{8,12},{12,16},{16,20},{20,24},{24,28},{1,5},{5,9},{9,... | collective-permute-start | bytes 200 | tf_op jit(solution)/shard_map/ppermute | solution.py:18
  69.4 2.5 %collective-permute-start.4 = (f32[16]{0:T(128)S(1)}, f32[16]{0:T(128)S(1)}, u32[]{:S(2)}, u32[]{:S(2)}) collective-permute-start(f32[16]{0:T(128)S(1)} %collective-permute-done.2), channel_id=1, source_target_pairs={{0,4},{4,8},{8,12},{12,16},{16,20},{20,24},{24,28},{1,5},{5,9},{9,... | collective-permute-start | bytes 200 | tf_op jit(solution)/shard_map/ppermute | solution.py:18
  72.9 6.5 %collective-permute-start.5 = (bf16[16,64,128]{2,1,0:T(8,128)(2,1)S(1)}, bf16[16,64,128]{2,1,0:T(8,128)(2,1)S(1)}, u32[]{:S(2)}, u32[]{:S(2)}) collective-permute-start(bf16[16,64,128]{2,1,0:T(8,128)(2,1)S(1)} %fusion.72), channel_id=1, source_target_pairs={{0,8},{4,12},{8,16},{12,20},{16,24},{20,28},{1,9},{5,13},{9,17},{1... | collective-permute-start | bytes 786440 | tf_op jit(solution)/shard_map/ppermute | solution.py:18
  79.4 4.6 %collective-permute-done.5 = bf16[16,64,128]{2,1,0:T(8,128)(2,1)S(1)} collective-permute-done((bf16[16,64,128]{2,1,0:T(8,128)(2,1)S(1)}, bf16[16,64,128]{2,1,0:T(8,128)(2,1)S(1)}, u32[]{:S(2)}, u32[]{:S(2)}) %collective-permute-start.5) | collective-permute-done | bytes 262176 | tf_op jit(solution)/shard_map/ppermute | solution.py:18
  84.3 5.4 %collective-permute-start.7 = (bf16[16,64,128]{2,1,0:T(8,128)(2,1)S(1)}, bf16[16,64,128]{2,1,0:T(8,128)(2,1)S(1)}, u32[]{:S(2)}, u32[]{:S(2)}) collective-permute-start(bf16[16,64,128]{2,1,0:T(8,128)(2,1)S(1)} %fusion.74), channel_id=1, source_target_pairs={{0,16},{4,20},{8,24},{12,28},{1,17},{5,21},{9,25},{13,29},{2,18},{... | collective-permute-start | bytes 786440 | tf_op jit(solution)/shard_map/ppermute | solution.py:18
  89.7 2.4 %collective-permute-start.6 = (f32[16]{0:T(128)S(1)}, f32[16]{0:T(128)S(1)}, u32[]{:S(2)}, u32[]{:S(2)}) collective-permute-start(f32[16]{0:T(128)S(1)} %get-tuple-element.77), channel_id=1, source_target_pairs={{0,8},{4,12},{8,16},{12,20},{16,24},{20,28},{1,9},{5,13},{9,17},{1... | collective-permute-start | bytes 200 | tf_op jit(solution)/shard_map/ppermute | solution.py:18
  92.2 2.0 collective-permute-done.6
  94.2 1.2 multiply_add_fusion
  95.3 31.1 %all-gather.6.cloned.1.call-done = bf16[2,768,2048]{2,1,0:T(8,128)(2,1)} async-done(((bf16[2,768,512]{2,1,0:T(8,128)(2,1)}), bf16[2,768,2048]{2,1,0:T(8,128)(2,1)}) %all-gather.6.cloned.1.call-update) | async-done | bytes 6291472 | tf_op jit(solution)/shard_map/all_gather | solution.py:180
  126.4 5.3 %fusion.101 = f32[2,768,256]{2,1,0:T(8,128)S(1)} fusion(bf16[2,768,2048]{2,1,0:T(8,128)(2,1)} %all-gather.6.cloned.1.call-done, bf16[2,2048,256]{2,1,0:T(8,128)(2,1)} %param.42), kind=kOutput, calls=%fused_computation.161 | convolution fusion | flops 1610612736 | bytes 9961472 | tf_op jit(solution)/shard_map/esd,edf->esf/dot_general | solution.py:197
  132.2 2.9 %multiply_convert_fusion = bf16[2,768,256]{2,1,0:T(8,128)(2,1)} fusion(f32[2,768,256]{2,1,0:T(8,128)S(1)} %fusion.101, bf16[2,768,2048]{2,1,0:T(8,128)(2,1)S(1)} %copy-done.33, bf16[2,2048,256]{2,1,0:T(8,128)(2,1)S(1)} %copy-done.35), kind=kOutput, calls=%fused_computation.25 | convolution fusion | flops 1612972032 | bytes 10747904 | tf_op jit(solution)/shard_map/esd,edf->esf/dot_general | solution.py:200
  136.8 1.6 copy.93
  138.4 2.0 copy.95
  141.1 1.8 fusion.100
  146.3 4.2 %fusion.27 = f32[2,128,16,64]{1,3,2,0:T(8,128)S(1)} fusion(f32[2,128,16,128]{3,1,2,0:T(8,128)S(1)} %bitcast.121, f32[2,16,64,128]{3,2,1,0:T(8,128)S(1)} %copy-done.11, f32[2,128,16]{1,2,0:T(8,128)S(1)} %copy-done.13, f32[16,64,128]{2,1,0:T(8,128)S(1)} %copy-done.9, f32[2,16]{1,0:T(2,128)S(1)} %copy-done.27), kind=kOutput, calls=%fused_computation.37 | convolution fusion | flops 403439616 | bytes 4735104 | tf_op jit(solution)/shard_map/bihn,bhpn->bihp/dot_general | solution.py:184
  151.7 4.2 %fusion.24 = f32[2,128,16,64]{1,3,2,0:T(8,128)S(1)} fusion(f32[2,128,16,64]{1,3,2,0:T(8,128)S(1)} %fusion.27, f32[2,16,128,128]{3,2,1,0:T(8,128)S(1)} %bitcast.119, f32[2,128,16,64]{1,0,3,2:T(2,128)S(1)} %copy-done.6, f32[2,16,128]{2,1,0:T(8,128)S(1)} %copy.85, pred[128,128]{1,0:T(8,128)(4,1)S(1)} %copy-done.12), kind=kOutput, calls=%fused_computation.35 | convolution fusion | flops 405012480 | bytes 5275648 | tf_op jit(solution)/shard_map/bhij,bjhp->bihp/dot_general | solution.py:151
  155.9 1.8 copy.94
  157.7 3.2 %reshape.140 = f32[256,4,256]{0,2,1:T(8,128)} reshape(f32[2,128,16,64]{1,0,3,2:T(2,128)} %copy.94) | data formatting | bytes 2097152 | tf_op jit(solution)/shard_map/reshape | solution.py:187
  160.9 2.0 multiply_reduce_fusion
  164.4 14.7 %all-gather.10.cloned.1.call-done = bf16[2,768,1024]{2,1,0:T(8,128)(2,1)} async-done(((bf16[2,768,256]{2,1,0:T(8,128)(2,1)}), bf16[2,768,1024]{2,1,0:T(8,128)(2,1)}) %all-gather.10.cloned.1.call-update) | async-done | bytes 3145744 | tf_op jit(solution)/shard_map/all_gather | solution.py:208
  179.0 3.7 %convolution_convert_fusion = bf16[2,768,512]{2,1,0:T(8,128)(2,1)S(1)} fusion(bf16[2,768,1024]{2,1,0:T(8,128)(2,1)} %all-gather.10.cloned.1.call-done, bf16[2,1024,512]{2,1,0:T(8,128)(2,1)S(1)} %copy-done), kind=kOutput, calls=%fused_computation.21 | convolution fusion | flops 1611399168 | bytes 6815744 | tf_op jit(solution)/shard_map/esf,efd->esd/dot_general | solution.py:217
  183.0 1.3 pad_maximum_fusion.1
  184.4 4.7 %all-to-all-start = ((bf16[8,192,512]{2,1,0:T(8,128)(2,1)}), bf16[8,192,512]{2,1,0:T(8,128)(2,1)}, u32[]{:S(2)}, u32[]{:S(2)}) async-start(bf16[8,192,512]{2,1,0:T(8,128)(2,1)} %pad_maximum_fusion.1), calls=%async_computation | async-start | bytes 3145728 | tf_op jit(solution)/shard_map/all_to_all | solution.py:224
  189.4 30.9 %all-gather.8.cloned.1.call-done = bf16[256,5120]{0,1:T(8,128)(2,1)} async-done(((bf16[256,1280]{0,1:T(8,128)(2,1)}), bf16[256,5120]{0,1:T(8,128)(2,1)}) %all-gather.8.cloned.1.call-update) | async-done | bytes 2621456 | tf_op jit(solution)/shard_map/all_gather | solution.py:209
  220.3 1.1 slice.201
  221.4 1.9 slice.194
  224.2 2.0 convolution_convert_fusion.1
  227.0 2.4 %fusion.47 = f32[256,512]{1,0:T(8,128)S(1)} fusion(bf16[1536,512]{1,0:T(8,128)(2,1)} %bitcast.43, f32[256]{0:T(256)S(1)} %bitcast.151, s32[256]{0:T(256)S(1)} %bitcast.157, f32[256]{0:T(256)S(1)} %bitcast.153, s32[256]{0:T(256)S(1)} %bitcast.159, f32[256]{0:T(256)S(1)} %bitcast.149, s32[256]{0:T(256)S(1)} %bitcast.161, f32[256]{0:T(256)S(1)} %bitcast.147, ...), kind=kOutput, calls=%fused_computation.70 | convolution fusion | flops 407764992 | bytes 2105344 | tf_op jit(solution)/shard_map/dot_general | solution.py:239
  229.5 2.6 %convolution_add_fusion.1 = f32[256,512]{1,0:T(8,128)S(1)} fusion(f32[256,512]{1,0:T(8,128)S(1)} %fusion.47, bf16[1536,512]{1,0:T(8,128)(2,1)} %bitcast.43, f32[256]{0:T(256)S(1)} %bitcast.152, s32[256]{0:T(256)S(1)} %bitcast.158, f32[256]{0:T(256)S(1)} %bitcast.154, s32[256]{0:T(256)S(1)} %bitcast.160, f32[256]{0:T(256)S(1)} %bitcast.150, ...), kind=kOutput, calls=%fused_computation.41 | convolution fusion | flops 408289280 | bytes 2629632 | tf_op jit(solution)/shard_map/dot_general | solution.py:241
  232.1 1.2 fusion.28
  (161 shorter events, 31.9 us)
Async XLA Ops:
  7.2 171.9 %copy-start = (bf16[2,1024,512]{2,1,0:T(8,128)(2,1)S(1)}, bf16[2,1024,512]{2,1,0:T(8,128)(2,1)}, u32[]{:S(2)}) copy-start(bf16[2,1024,512]{2,1,0:T(8,128)(2,1)} %param.44) | copy-start | bytes 6291460
  7.2 8.8 %copy-start.7 = (bf16[256,2048]{1,0:T(8,128)(2,1)S(1)}, bf16[256,2048]{1,0:T(8,128)(2,1)}, u32[]{:S(2)}) copy-start(bf16[256,2048]{1,0:T(8,128)(2,1)} %param.38) | copy-start | bytes 3145732
  7.2 8.2 %copy-start.17 = (s32[256,4]{0,1:T(4,128)S(1)}, s32[256,4]{0,1:T(4,128)}, u32[]{:S(2)}) copy-start(s32[256,4]{0,1:T(4,128)} %param.40) | copy-start | bytes 12292
  7.2 8.8 %copy-start.22 = (f32[2048]{0:T(1024)S(1)}, f32[2048]{0:T(1024)}, u32[]{:S(2)}) copy-start(f32[2048]{0:T(1024)} %param.39) | copy-start | bytes 24580
  7.2 42.7 %all-gather.12.cloned.1.call-start = ((), (), s32[]{:S(2)}) async-start(), calls=%async_computation.4 | async-start | bytes 2433024 | tf_op jit(solution)/shard_map/all_gather | solution.py:133
  10.7 14.2 %collective-permute-start = (bf16[3,2048]{0,1:T(8,128)(2,1)}, bf16[3,2048]{0,1:T(8,128)(2,1)}, u32[]{:S(2)}, u32[]{:S(2)}) collective-permute-start(bf16[3,2048]{0,1:T(8,128)(2,1)} %copy.77), channel_id=1, source_target_pairs={{0,4},{4,8},{8,12},{12,16},{16,20},{20,24},{24,28},{1,5},{5,9},{9,... | collective-permute-start | bytes 36872 | tf_op jit(solution)/shard_map/ppermute | solution.py:18
  16.0 2.3 copy-start.37
  16.0 2.3 copy-start.23
  16.0 2.9 %copy-start.20 = (f32[256,16]{0,1:T(8,128)S(1)}, f32[256,16]{0,1:T(8,128)}, u32[]{:S(2)}) copy-start(f32[256,16]{0,1:T(8,128)} %param.29) | copy-start | bytes 49156
  16.1 2.9 %copy-start.21 = (f32[256,16]{0,1:T(8,128)S(1)}, f32[256,16]{0,1:T(8,128)}, u32[]{:S(2)}) copy-start(f32[256,16]{0,1:T(8,128)} %param.30) | copy-start | bytes 49156
  16.1 4.4 %copy-start.24 = (f32[4,512]{1,0:T(4,128)S(1)}, f32[4,512]{1,0:T(4,128)}, u32[]{:S(2)}) copy-start(f32[4,512]{1,0:T(4,128)} %param.35) | copy-start | bytes 24580
  16.1 5.0 %copy-start.19 = (f32[4,1024]{1,0:T(4,128)S(1)}, f32[4,1024]{1,0:T(4,128)}, u32[]{:S(2)}) copy-start(f32[4,1024]{1,0:T(4,128)} %param.33) | copy-start | bytes 49156
  18.2 108.2 %all-gather.6.cloned.1.call-start = ((), (), s32[]{:S(2)}) async-start(), calls=%async_computation.1 | async-start | bytes 7864320 | tf_op jit(solution)/shard_map/all_gather | solution.py:180
  38.6 3.0 %copy-start.8 = (f32[2,128,4,128]{3,1,2,0:T(8,128)S(1)}, f32[2,128,4,128]{3,1,2,0:T(8,128)}, u32[]{:S(2)}) copy-start(f32[2,128,4,128]{3,1,2,0:T(8,128)} %copy.89) | copy-start | bytes 1572868
  41.8 3.1 %copy-start.28 = (f32[2,16]{1,0:T(2,128)S(1)}, f32[2,16]{1,0:T(2,128)}, u32[]{:S(2)}) copy-start(f32[2,16]{1,0:T(2,128)} %get-tuple-element.151) | copy-start | bytes 388
  44.9 5.9 %copy-start.29 = (f32[2]{0:T(128)S(1)}, f32[2]{0:T(128)}, u32[]{:S(2)}) copy-start(f32[2]{0:T(128)} %add_convert_fusion) | copy-start | bytes 28
  51.3 2.3 copy-start.32
  55.4 8.8 %copy-start.31 = (f32[16]{0:T(128)S(1)}, f32[16]{0:T(128)}, u32[]{:S(2)}) copy-start(f32[16]{0:T(128)} %get-tuple-element.84) | copy-start | bytes 196
  55.4 123.6 %all-gather.10.cloned.1.call-start = ((), (), s32[]{:S(2)}) async-start(), calls=%async_computation.3 | async-start | bytes 3932160 | tf_op jit(solution)/shard_map/all_gather | solution.py:208
  55.5 4.1 %collective-permute-start.1 = (bf16[16,64,128]{2,1,0:T(8,128)(2,1)S(1)}, bf16[16,64,128]{2,1,0:T(8,128)(2,1)S(1)}, u32[]{:S(2)}, u32[]{:S(2)}) collective-permute-start(bf16[16,64,128]{2,1,0:T(8,128)(2,1)S(1)} %convert_element_type.179), channel_id=1, source_target_pairs={{0,4},{4,8},{8,12},{12,16},{16,20},{20,24},{24,28},{1,5},{5,9},{9,... | collective-permute-start | bytes 786440 | tf_op jit(solution)/shard_map/ppermute | solution.py:18
  59.7 13.1 %collective-permute-start.3 = (bf16[16,64,128]{2,1,0:T(8,128)(2,1)S(1)}, bf16[16,64,128]{2,1,0:T(8,128)(2,1)S(1)}, u32[]{:S(2)}, u32[]{:S(2)}) collective-permute-start(bf16[16,64,128]{2,1,0:T(8,128)(2,1)S(1)} %collective-permute-done.1), channel_id=1, source_target_pairs={{0,4},{4,8},{8,12},{12,16},{16,20},{20,24},{24,28},{1,5},{5,9},{9,... | collective-permute-start | bytes 786440 | tf_op jit(solution)/shard_map/ppermute | solution.py:18
  64.2 5.2 %collective-permute-start.2 = (f32[16]{0:T(128)S(1)}, f32[16]{0:T(128)S(1)}, u32[]{:S(2)}, u32[]{:S(2)}) collective-permute-start(f32[16]{0:T(128)S(1)} %copy-done.31), channel_id=1, source_target_pairs={{0,4},{4,8},{8,12},{12,16},{16,20},{20,24},{24,28},{1,5},{5,9},{9,... | collective-permute-start | bytes 200 | tf_op jit(solution)/shard_map/ppermute | solution.py:18
  69.4 3.3 %collective-permute-start.4 = (f32[16]{0:T(128)S(1)}, f32[16]{0:T(128)S(1)}, u32[]{:S(2)}, u32[]{:S(2)}) collective-permute-start(f32[16]{0:T(128)S(1)} %collective-permute-done.2), channel_id=1, source_target_pairs={{0,4},{4,8},{8,12},{12,16},{16,20},{20,24},{24,28},{1,5},{5,9},{9,... | collective-permute-start | bytes 200 | tf_op jit(solution)/shard_map/ppermute | solution.py:18
  72.9 11.1 %collective-permute-start.5 = (bf16[16,64,128]{2,1,0:T(8,128)(2,1)S(1)}, bf16[16,64,128]{2,1,0:T(8,128)(2,1)S(1)}, u32[]{:S(2)}, u32[]{:S(2)}) collective-permute-start(bf16[16,64,128]{2,1,0:T(8,128)(2,1)S(1)} %fusion.72), channel_id=1, source_target_pairs={{0,8},{4,12},{8,16},{12,20},{16,24},{20,28},{1,9},{5,13},{9,17},{1... | collective-permute-start | bytes 786440 | tf_op jit(solution)/shard_map/ppermute | solution.py:18
  84.3 9.9 %collective-permute-start.7 = (bf16[16,64,128]{2,1,0:T(8,128)(2,1)S(1)}, bf16[16,64,128]{2,1,0:T(8,128)(2,1)S(1)}, u32[]{:S(2)}, u32[]{:S(2)}) collective-permute-start(bf16[16,64,128]{2,1,0:T(8,128)(2,1)S(1)} %fusion.74), channel_id=1, source_target_pairs={{0,16},{4,20},{8,24},{12,28},{1,17},{5,21},{9,25},{13,29},{2,18},{... | collective-permute-start | bytes 786440 | tf_op jit(solution)/shard_map/ppermute | solution.py:18
  89.7 4.5 %collective-permute-start.6 = (f32[16]{0:T(128)S(1)}, f32[16]{0:T(128)S(1)}, u32[]{:S(2)}, u32[]{:S(2)}) collective-permute-start(f32[16]{0:T(128)S(1)} %get-tuple-element.77), channel_id=1, source_target_pairs={{0,8},{4,12},{8,16},{12,20},{16,24},{20,28},{1,9},{5,13},{9,17},{1... | collective-permute-start | bytes 200 | tf_op jit(solution)/shard_map/ppermute | solution.py:18
  126.4 5.4 %copy-start.33 = (bf16[2,768,2048]{2,1,0:T(8,128)(2,1)S(1)}, bf16[2,768,2048]{2,1,0:T(8,128)(2,1)}, u32[]{:S(2)}) copy-start(bf16[2,768,2048]{2,1,0:T(8,128)(2,1)} %all-gather.6.cloned.1.call-done) | copy-start | bytes 18874372
  126.4 5.8 %copy-start.35 = (bf16[2,2048,256]{2,1,0:T(8,128)(2,1)S(1)}, bf16[2,2048,256]{2,1,0:T(8,128)(2,1)}, u32[]{:S(2)}) copy-start(bf16[2,2048,256]{2,1,0:T(8,128)(2,1)} %param.43) | copy-start | bytes 6291460
  132.2 3.0 %copy-start.30 = (f32[16]{0:T(128)S(1)}, f32[16]{0:T(128)}, u32[]{:S(2)}) copy-start(f32[16]{0:T(128)} %param.32) | copy-start | bytes 196
  135.1 5.9 %copy-start.4 = (bf16[256,2048]{1,0:T(8,128)(2,1)S(1)}, bf16[256,2048]{1,0:T(8,128)(2,1)}, u32[]{:S(2)}) copy-start(bf16[256,2048]{1,0:T(8,128)(2,1)} %copy-done.3) | copy-start | bytes 3145732
  135.2 85.1 %all-gather.8.cloned.1.call-start = ((), (), s32[]{:S(2)}) async-start(), calls=%async_computation.2 | async-start | bytes 3276800 | tf_op jit(solution)/shard_map/all_gather | solution.py:209
  140.4 2.5 %copy-start.36 = (bf16[2048,256]{1,0:T(8,128)(2,1)S(1)}, bf16[2048,256]{1,0:T(8,128)(2,1)}, u32[]{:S(2)}) copy-start(bf16[2048,256]{1,0:T(8,128)(2,1)} %param.46) | copy-start | bytes 3145732
  144.8 1.4 copy-start.11
  144.9 1.4 copy-start.13
  144.9 1.4 copy-start.27
  150.4 1.2 copy-start.6
  157.7 3.2 %copy-start.1 = (f32[256,1024]{0,1:T(8,128)S(1)}, f32[256,1024]{0,1:T(8,128)}, u32[]{:S(2)}) copy-start(f32[256,1024]{0,1:T(8,128)} %fusion.71) | copy-start | bytes 3145732
  157.7 3.2 %copy-start.16 = (f32[4,256]{1,0:T(4,128)S(1)}, f32[4,256]{1,0:T(4,128)}, u32[]{:S(2)}) copy-start(f32[4,256]{1,0:T(4,128)} %mul.377) | copy-start | bytes 12292
  160.9 2.0 copy-start.2
  160.9 2.0 copy-start.5
  160.9 2.0 copy-start.15
  160.9 2.0 copy-start.25
  184.4 4.8 %copy-start.14 = (f32[4,256]{1,0:T(4,128)S(1)}, f32[4,256]{1,0:T(4,128)}, u32[]{:S(2)}) copy-start(f32[4,256]{1,0:T(4,128)} %get-tuple-element.110) | copy-start | bytes 12292
  184.4 5.0 %copy-start.26 = (f32[256,4]{0,1:T(4,128)S(1)}, f32[256,4]{0,1:T(4,128)}, u32[]{:S(2)}) copy-start(f32[256,4]{0,1:T(4,128)} %param.41) | copy-start | bytes 12292
  184.4 5.0 %copy-start.18 = (s32[256,4]{0,1:T(4,128)S(1)}, s32[256,4]{0,1:T(4,128)}, u32[]{:S(2)}) copy-start(s32[256,4]{0,1:T(4,128)} %param.40) | copy-start | bytes 12292
  184.4 42.6 %all-to-all-start = ((bf16[8,192,512]{2,1,0:T(8,128)(2,1)}), bf16[8,192,512]{2,1,0:T(8,128)(2,1)}, u32[]{:S(2)}, u32[]{:S(2)}) async-start(bf16[8,192,512]{2,1,0:T(8,128)(2,1)} %pad_maximum_fusion.1), calls=%async_computation | async-start | bytes 3145728 | tf_op jit(solution)/shard_map/all_to_all | solution.py:224
  221.3 2.8 %copy-start.34 = (bf16[4096,512]{1,0:T(8,128)(2,1)S(1)}, bf16[4096,512]{1,0:T(8,128)(2,1)}, u32[]{:S(2)}) copy-start(bf16[4096,512]{1,0:T(8,128)(2,1)} %param.37) | copy-start | bytes 12582916
  229.5 2.6 %copy-start.10 = (bf16[1024,512]{1,0:T(8,128)(2,1)S(1)}, bf16[1024,512]{1,0:T(8,128)(2,1)}, u32[]{:S(2)}) copy-start(bf16[1024,512]{1,0:T(8,128)(2,1)} %param.47) | copy-start | bytes 3145732
  (3 other events, 3.4 us)
Sparse Core Ops, SparseCore 0:
  18.4 31.4 all-gather.11
  55.5 70.8 all-gather.5
  135.3 43.6 all-gather.9
  180.7 39.4 all-gather.7
where the time goes:
time: 241 us; the launch traced here: 240 us
  waiting for transfers between devices  87.8 us (36%)
  matrix products  37.4 us (16%)
  starting transfers between devices  36.9 us (15%)
  local copies, waits for them, and re-layouts  34.6 us (14%)
  other arithmetic  28.6 us (12%)
  between operations  14.4 us (6%)
    ppermute x8, starting transfers between devices, passed_along(): return lax.ppermute(x, axis, pairs)  32 us
    all_gather x1, waiting for transfers between devices, on_device(): column_piece = lax.all_gather(arrived, 'tp', axis=2, tiled=True)  31.1 us
    all_gather x1, waiting for transfers between devices, on_device(): lax.all_gather(jnp.concatenate([mixer_normed, shared_hidden], axis=1), 't...  30.9 us
    all_gather x1, waiting for transfers between devices, on_device(): whole_hidden = lax.all_gather(hidden, 'tp', axis=2, tiled=True)  14.7 us
    ppermute x8, waiting for transfers between devices, passed_along(): return lax.ppermute(x, axis, pairs)  9.39 us
    unnamed x77, local copies, waits for them, and re-layouts  6.78 us
    dot_general x1, matrix products, on_device(): jnp.einsum('esd,edf->esf', column_piece, routed_gate_weight, preferred_el...  5.34 us
  transfers between devices with their start and end apart: 13, of which 10 were waited for; matrix products, arithmetic and copies ran while one was open for 30% of the time, Pallas kernels for 0%

commit v1 on v0

--- a/solution.py
+++ b/solution.py
@@ -177,7 +177,8 @@
             for j in range(local_experts)
         ]
     )
-    column_piece = lax.all_gather(arrived, "tp", axis=2, tiled=True)
+    blocks = lax.all_gather(arrived, "tp")
+    column_piece = jnp.concatenate(blocks, axis=2)
     column_piece, incoming = lax.optimization_barrier((column_piece, incoming))
     entering = local_prev + jnp.exp(before_logs)[:, :, None, None] * incoming[None]
     carried_term = (

time: 241 us -> 241 us (level)
  matrix products: 37.4 us -> 33.9 us
  local copies, waits for them, and re-layouts: 34.6 us -> 38.1 us
    reshape x0 -> x1, local copies, waits for them, and re-layouts: none -> 3.9 us  [on_device(): column_piece = jnp.concatenate(blocks, axis=2)]
    dot_general x1, matrix products: 5.34 us -> 1.79 us  [on_device(): jnp.einsum('esd,edf->esf', column_piece, routed_gate_weight, preferred_el...]
where the time goes in v1:
time: 241 us; the launch traced here: 240 us
  waiting for transfers between devices  88 us (37%)
  local copies, waits for them, and re-layouts  38.1 us (16%)
  starting transfers between devices  36.8 us (15%)
  matrix products  33.9 us (14%)
  other arithmetic  28.6 us (12%)
  between operations  14.5 us (6%)
    ppermute x8, starting transfers between devices, passed_along(): return lax.ppermute(x, axis, pairs)  32 us
    all_gather x1, waiting for transfers between devices, on_device(): blocks = lax.all_gather(arrived, 'tp')  31.2 us
    all_gather x1, waiting for transfers between devices, on_device(): lax.all_gather(jnp.concatenate([mixer_normed, shared_hidden], axis=1), 't...  30.9 us
    all_gather x1, waiting for transfers between devices, on_device(): whole_hidden = lax.all_gather(hidden, 'tp', axis=2, tiled=True)  14.7 us
    ppermute x8, waiting for transfers between devices, passed_along(): return lax.ppermute(x, axis, pairs)  9.39 us
    unnamed x77, local copies, waits for them, and re-layouts  6.33 us
  transfers between devices with their start and end apart: 13, of which 10 were waited for; matrix products, arithmetic and copies ran while one was open for 30% of the time, Pallas kernels for 0%

profile of v1, /device:TPU:0, one launch (start us, length us, event | category | flops | bytes accessed | tf_op | source)
XLA Modules:
  0.0 239.8 jit_solution(16747885393225792839)
XLA Ops:
  9.6 1.1 copy.80
  10.7 3.2 %collective-permute-start = (bf16[3,2048]{0,1:T(8,128)(2,1)}, bf16[3,2048]{0,1:T(8,128)(2,1)}, u32[]{:S(2)}, u32[]{:S(2)}) collective-permute-start(bf16[3,2048]{0,1:T(8,128)(2,1)} %copy.80), channel_id=1, source_target_pairs={{0,4},{4,8},{8,12},{12,16},{16,20},{20,24},{24,28},{1,5},{5,9},{9,... | collective-permute-start | bytes 36872 | tf_op jit(solution)/shard_map/ppermute | solution.py:18
  13.9 1.5 fusion.1
  23.6 1.3 copy.81
  26.7 3.4 %multiply_convert_fusion.2 = (bf16[256,512]{1,0:T(8,128)(2,1)}, bf16[256,512]{1,0:T(8,128)(2,1)}) fusion(bf16[256,512]{1,0:T(8,128)(2,1)} %param.26, bf16[3,512]{1,0:T(4,128)(2,1)} %copy.84, f32[512]{0:T(512)} %bitcast.149, f32[512]{0:T(512)} %bitcast.150, f32[512]{0:T(512)} %bitcast.148, f32[512]{0:T(512)} %bitcast.147, f32[512]{0:T(512)} %bitcast.153, ...), kind=kLoop, calls=%fused_computation.103 | loop fusion | flops 6553600 | bytes 1071104 | tf_op jit(solution)/shard_map/convert_element_type | solution.py:44
  32.9 2.9 %fusion.71 = f32[256,1024]{0,1:T(8,128)} fusion(f32[1024]{0:T(1024)} %bitcast.142, bf16[256,1024]{0,1:T(8,128)(2,1)S(1)} %copy.81, f32[1024]{0:T(1024)} %bitcast.143, bf16[3,1024]{0,1:T(8,128)(2,1)S(1)} %slice.176, f32[1024]{0:T(1024)} %bitcast.141, f32[1024]{0:T(1024)} %bitcast.140), kind=kLoop, calls=%fused_computation.106 | loop fusion | flops 6815744 | bytes 1595392 | tf_op jit(solution)/shard_map/convert_element_type | solution.py:140
  35.8 2.7 %reshape.138 = f32[2,128,16,64]{1,0,3,2:T(2,128)} reshape(f32[256,1024]{0,1:T(8,128)} %fusion.71) | data formatting | bytes 2097152 | tf_op jit(solution)/shard_map/reshape | solution.py:140
  38.6 3.0 %broadcast_multiply_fusion = (f32[2,128,16,64]{1,0,3,2:T(2,128)S(1)}, f32[2,128,16,64]{1,0,3,2:T(2,128)}) fusion(f32[2,128,16]{1,0,2:T(2,128)S(1)} %copy.91, f32[2,128,16,64]{1,0,3,2:T(2,128)} %reshape.138, f32[2,128,16]{1,0,2:T(2,128)} %mul.326), kind=kLoop, calls=%fused_computation.102 | loop fusion | flops 524288 | bytes 3178496 | tf_op jit(solution)/shard_map/bjhn,bjh,bjhp->bhpn/dot_general | solution.py:156
  41.8 3.1 %fusion.37 = f32[2,16,64,128]{3,2,1,0:T(8,128)} fusion(f32[2,128,16,128]{3,1,2,0:T(8,128)S(1)} %bitcast.125, f32[2,128,16,64]{1,0,3,2:T(2,128)S(1)} %get-tuple-element.78), kind=kOutput, calls=%fused_computation.55 | convolution fusion | flops 402653184 | bytes 4194304 | tf_op jit(solution)/shard_map/bjhn,bjh,bjhp->bhpn/dot_general | solution.py:156
  44.9 4.0 %while.13 = (s32[]{:T(128)}, f32[16,64,128]{2,1,0:T(8,128)S(1)}, f32[2,16,64,128]{3,2,1,0:T(8,128)}, f32[2,16]{1,0:T(2,128)S(1)}, f32[2,16,64,128]{3,2,1,0:T(8,128)}, /*index=5*/s32[]{:T(128)}, s32[]{:T(128)}) while((s32[]{:T(128)}, f32[16,64,128]{2,1,0:T(8,128)S(1)}, f32[2,16,64,128]{3,2,1,0:T(8,128)}, f32[2,16]{1,0:T(2,128)S(1)}, ...), condition=%wide.region_3.4_spmd.clone, body=%wide.region_2.3_spmd.clone.sunk | while | flops 524291 | bytes 2621740 | solution.py:158
  45.8 1.2 bitcast_add_fusion.4
  47.8 1.2 bitcast_add_fusion.4
  51.3 2.3 fusion.18
  54.0 1.3 pad_maximum_fusion
  55.5 3.0 %collective-permute-start.1 = (bf16[16,64,128]{2,1,0:T(8,128)(2,1)S(1)}, bf16[16,64,128]{2,1,0:T(8,128)(2,1)S(1)}, u32[]{:S(2)}, u32[]{:S(2)}) collective-permute-start(bf16[16,64,128]{2,1,0:T(8,128)(2,1)S(1)} %convert_element_type.179), channel_id=1, source_target_pairs={{0,4},{4,8},{8,12},{12,16},{16,20},{20,24},{24,28},{1,5},{5,9},{9,... | collective-permute-start | bytes 786440 | tf_op jit(solution)/shard_map/ppermute | solution.py:18
  58.5 1.1 collective-permute-done.1
  59.7 4.5 %collective-permute-start.3 = (bf16[16,64,128]{2,1,0:T(8,128)(2,1)S(1)}, bf16[16,64,128]{2,1,0:T(8,128)(2,1)S(1)}, u32[]{:S(2)}, u32[]{:S(2)}) collective-permute-start(bf16[16,64,128]{2,1,0:T(8,128)(2,1)S(1)} %collective-permute-done.1), channel_id=1, source_target_pairs={{0,4},{4,8},{8,12},{12,16},{16,20},{20,24},{24,28},{1,5},{5,9},{9,... | collective-permute-start | bytes 786440 | tf_op jit(solution)/shard_map/ppermute | solution.py:18
  64.2 4.4 %collective-permute-start.2 = (f32[16]{0:T(128)S(1)}, f32[16]{0:T(128)S(1)}, u32[]{:S(2)}, u32[]{:S(2)}) collective-permute-start(f32[16]{0:T(128)S(1)} %copy-done.31), channel_id=1, source_target_pairs={{0,4},{4,8},{8,12},{12,16},{16,20},{20,24},{24,28},{1,5},{5,9},{9,... | collective-permute-start | bytes 200 | tf_op jit(solution)/shard_map/ppermute | solution.py:18
  69.4 2.5 %collective-permute-start.4 = (f32[16]{0:T(128)S(1)}, f32[16]{0:T(128)S(1)}, u32[]{:S(2)}, u32[]{:S(2)}) collective-permute-start(f32[16]{0:T(128)S(1)} %collective-permute-done.2), channel_id=1, source_target_pairs={{0,4},{4,8},{8,12},{12,16},{16,20},{20,24},{24,28},{1,5},{5,9},{9,... | collective-permute-start | bytes 200 | tf_op jit(solution)/shard_map/ppermute | solution.py:18
  72.9 6.5 %collective-permute-start.5 = (bf16[16,64,128]{2,1,0:T(8,128)(2,1)S(1)}, bf16[16,64,128]{2,1,0:T(8,128)(2,1)S(1)}, u32[]{:S(2)}, u32[]{:S(2)}) collective-permute-start(bf16[16,64,128]{2,1,0:T(8,128)(2,1)S(1)} %fusion.72), channel_id=1, source_target_pairs={{0,8},{4,12},{8,16},{12,20},{16,24},{20,28},{1,9},{5,13},{9,17},{1... | collective-permute-start | bytes 786440 | tf_op jit(solution)/shard_map/ppermute | solution.py:18
  79.4 4.6 %collective-permute-done.5 = bf16[16,64,128]{2,1,0:T(8,128)(2,1)S(1)} collective-permute-done((bf16[16,64,128]{2,1,0:T(8,128)(2,1)S(1)}, bf16[16,64,128]{2,1,0:T(8,128)(2,1)S(1)}, u32[]{:S(2)}, u32[]{:S(2)}) %collective-permute-start.5) | collective-permute-done | bytes 262176 | tf_op jit(solution)/shard_map/ppermute | solution.py:18
  84.3 5.4 %collective-permute-start.7 = (bf16[16,64,128]{2,1,0:T(8,128)(2,1)S(1)}, bf16[16,64,128]{2,1,0:T(8,128)(2,1)S(1)}, u32[]{:S(2)}, u32[]{:S(2)}) collective-permute-start(bf16[16,64,128]{2,1,0:T(8,128)(2,1)S(1)} %fusion.74), channel_id=1, source_target_pairs={{0,16},{4,20},{8,24},{12,28},{1,17},{5,21},{9,25},{13,29},{2,18},{... | collective-permute-start | bytes 786440 | tf_op jit(solution)/shard_map/ppermute | solution.py:18
  89.7 2.4 %collective-permute-start.6 = (f32[16]{0:T(128)S(1)}, f32[16]{0:T(128)S(1)}, u32[]{:S(2)}, u32[]{:S(2)}) collective-permute-start(f32[16]{0:T(128)S(1)} %get-tuple-element.77), channel_id=1, source_target_pairs={{0,8},{4,12},{8,16},{12,20},{16,24},{20,28},{1,9},{5,13},{9,17},{1... | collective-permute-start | bytes 200 | tf_op jit(solution)/shard_map/ppermute | solution.py:18
  92.2 2.0 collective-permute-done.6
  94.2 1.2 multiply_add_fusion
  95.3 31.2 %all-gather.13.cloned.1.call-done = bf16[8,768,512]{2,1,0:T(8,128)(2,1)} async-done(((bf16[2,768,512]{2,1,0:T(8,128)(2,1)}), bf16[8,768,512]{2,1,0:T(8,128)(2,1)}) %all-gather.13.cloned.1.call-update) | async-done | bytes 6291472 | tf_op jit(solution)/shard_map/all_gather | solution.py:180
  126.5 3.9 %copy.102 = bf16[4,2,96,8,512]{4,3,0,2,1:T(8,128)(2,1)S(1)} copy(bf16[4,2,96,8,512]{4,3,2,1,0:T(8,128)(2,1)} %bitcast.127) | data formatting | bytes 12582912 | tf_op jit(solution)/shard_map/reshape | solution.py:181
  130.5 1.8 fusion.101
  132.3 2.9 %multiply_convert_fusion = bf16[2,768,256]{2,1,0:T(8,128)(2,1)} fusion(f32[2,768,256]{2,1,0:T(8,128)S(1)} %fusion.101, bf16[2,768,2048]{2,1,0:T(8,128)(2,1)S(1)} %bitcast.129, bf16[2,2048,256]{2,1,0:T(8,128)(2,1)S(1)} %copy-done.35), kind=kOutput, calls=%fused_computation.25 | convolution fusion | flops 1612972032 | bytes 10747904 | tf_op jit(solution)/shard_map/esd,edf->esf/dot_general | solution.py:201
  136.9 1.6 copy.97
  138.4 2.0 copy.99
  141.1 1.8 fusion.100
  146.3 4.2 %fusion.27 = f32[2,128,16,64]{1,3,2,0:T(8,128)S(1)} fusion(f32[2,128,16,128]{3,1,2,0:T(8,128)S(1)} %bitcast.126, f32[2,16,64,128]{3,2,1,0:T(8,128)S(1)} %copy-done.11, f32[2,128,16]{1,2,0:T(8,128)S(1)} %copy-done.13, f32[16,64,128]{2,1,0:T(8,128)S(1)} %copy-done.9, f32[2,16]{1,0:T(2,128)S(1)} %copy-done.27), kind=kOutput, calls=%fused_computation.37 | convolution fusion | flops 403439616 | bytes 4735104 | tf_op jit(solution)/shard_map/bihn,bhpn->bihp/dot_general | solution.py:185
  151.7 4.3 %fusion.24 = f32[2,128,16,64]{1,3,2,0:T(8,128)S(1)} fusion(f32[2,128,16,64]{1,3,2,0:T(8,128)S(1)} %fusion.27, f32[2,16,128,128]{3,2,1,0:T(8,128)S(1)} %bitcast.124, f32[2,128,16,64]{1,0,3,2:T(2,128)S(1)} %copy-done.6, f32[2,16,128]{2,1,0:T(8,128)S(1)} %copy.88, pred[128,128]{1,0:T(8,128)(4,1)S(1)} %copy-done.12), kind=kOutput, calls=%fused_computation.35 | convolution fusion | flops 405012480 | bytes 5275648 | tf_op jit(solution)/shard_map/bhij,bjhp->bihp/dot_general | solution.py:151
  156.0 1.8 copy.98
  157.8 3.2 %reshape.148 = f32[256,4,256]{0,2,1:T(8,128)} reshape(f32[2,128,16,64]{1,0,3,2:T(2,128)} %copy.98) | data formatting | bytes 2097152 | tf_op jit(solution)/shard_map/reshape | solution.py:188
  161.0 2.0 multiply_reduce_fusion
  164.4 14.7 %all-gather.9.cloned.1.call-done = bf16[2,768,1024]{2,1,0:T(8,128)(2,1)} async-done(((bf16[2,768,256]{2,1,0:T(8,128)(2,1)}), bf16[2,768,1024]{2,1,0:T(8,128)(2,1)}) %all-gather.9.cloned.1.call-update) | async-done | bytes 3145744 | tf_op jit(solution)/shard_map/all_gather | solution.py:209
  179.1 3.7 %convolution_convert_fusion = bf16[2,768,512]{2,1,0:T(8,128)(2,1)S(1)} fusion(bf16[2,768,1024]{2,1,0:T(8,128)(2,1)} %all-gather.9.cloned.1.call-done, bf16[2,1024,512]{2,1,0:T(8,128)(2,1)S(1)} %copy-done), kind=kOutput, calls=%fused_computation.21 | convolution fusion | flops 1611399168 | bytes 6815744 | tf_op jit(solution)/shard_map/esf,efd->esd/dot_general | solution.py:218
  183.1 1.3 pad_maximum_fusion.1
  184.4 4.7 %all-to-all-start = ((bf16[8,192,512]{2,1,0:T(8,128)(2,1)}), bf16[8,192,512]{2,1,0:T(8,128)(2,1)}, u32[]{:S(2)}, u32[]{:S(2)}) async-start(bf16[8,192,512]{2,1,0:T(8,128)(2,1)} %pad_maximum_fusion.1), calls=%async_computation | async-start | bytes 3145728 | tf_op jit(solution)/shard_map/all_to_all | solution.py:225
  189.4 30.9 %all-gather.7.cloned.1.call-done = bf16[256,5120]{0,1:T(8,128)(2,1)} async-done(((bf16[256,1280]{0,1:T(8,128)(2,1)}), bf16[256,5120]{0,1:T(8,128)(2,1)}) %all-gather.7.cloned.1.call-update) | async-done | bytes 2621456 | tf_op jit(solution)/shard_map/all_gather | solution.py:210
  220.3 1.1 slice.201
  221.4 1.9 slice.194
  224.2 2.0 convolution_convert_fusion.1
  227.1 2.4 %fusion.47 = f32[256,512]{1,0:T(8,128)S(1)} fusion(bf16[1536,512]{1,0:T(8,128)(2,1)} %bitcast.45, f32[256]{0:T(256)S(1)} %bitcast.159, s32[256]{0:T(256)S(1)} %bitcast.165, f32[256]{0:T(256)S(1)} %bitcast.161, s32[256]{0:T(256)S(1)} %bitcast.167, f32[256]{0:T(256)S(1)} %bitcast.157, s32[256]{0:T(256)S(1)} %bitcast.169, f32[256]{0:T(256)S(1)} %bitcast.155, ...), kind=kOutput, calls=%fused_computation.70 | convolution fusion | flops 407764992 | bytes 2105344 | tf_op jit(solution)/shard_map/dot_general | solution.py:240
  229.5 2.6 %convolution_add_fusion.1 = f32[256,512]{1,0:T(8,128)S(1)} fusion(f32[256,512]{1,0:T(8,128)S(1)} %fusion.47, bf16[1536,512]{1,0:T(8,128)(2,1)} %bitcast.45, f32[256]{0:T(256)S(1)} %bitcast.160, s32[256]{0:T(256)S(1)} %bitcast.166, f32[256]{0:T(256)S(1)} %bitcast.162, s32[256]{0:T(256)S(1)} %bitcast.168, f32[256]{0:T(256)S(1)} %bitcast.158, ...), kind=kOutput, calls=%fused_computation.41 | convolution fusion | flops 408289280 | bytes 2629632 | tf_op jit(solution)/shard_map/dot_general | solution.py:242
  232.1 1.2 fusion.28
  (162 shorter events, 32.5 us)
Async XLA Ops:
  7.2 171.9 %copy-start = (bf16[2,1024,512]{2,1,0:T(8,128)(2,1)S(1)}, bf16[2,1024,512]{2,1,0:T(8,128)(2,1)}, u32[]{:S(2)}) copy-start(bf16[2,1024,512]{2,1,0:T(8,128)(2,1)} %param.44) | copy-start | bytes 6291460
  7.2 8.8 %copy-start.7 = (bf16[256,2048]{1,0:T(8,128)(2,1)S(1)}, bf16[256,2048]{1,0:T(8,128)(2,1)}, u32[]{:S(2)}) copy-start(bf16[256,2048]{1,0:T(8,128)(2,1)} %param.38) | copy-start | bytes 3145732
  7.2 8.2 %copy-start.17 = (s32[256,4]{0,1:T(4,128)S(1)}, s32[256,4]{0,1:T(4,128)}, u32[]{:S(2)}) copy-start(s32[256,4]{0,1:T(4,128)} %param.40) | copy-start | bytes 12292
  7.2 8.8 %copy-start.22 = (f32[2048]{0:T(1024)S(1)}, f32[2048]{0:T(1024)}, u32[]{:S(2)}) copy-start(f32[2048]{0:T(1024)} %param.39) | copy-start | bytes 24580
  7.2 42.7 %all-gather.11.cloned.1.call-start = ((), (), s32[]{:S(2)}) async-start(), calls=%async_computation.3 | async-start | bytes 2433024 | tf_op jit(solution)/shard_map/all_gather | solution.py:133
  10.7 14.2 %collective-permute-start = (bf16[3,2048]{0,1:T(8,128)(2,1)}, bf16[3,2048]{0,1:T(8,128)(2,1)}, u32[]{:S(2)}, u32[]{:S(2)}) collective-permute-start(bf16[3,2048]{0,1:T(8,128)(2,1)} %copy.80), channel_id=1, source_target_pairs={{0,4},{4,8},{8,12},{12,16},{16,20},{20,24},{24,28},{1,5},{5,9},{9,... | collective-permute-start | bytes 36872 | tf_op jit(solution)/shard_map/ppermute | solution.py:18
  16.0 2.3 copy-start.37
  16.0 2.3 copy-start.23
  16.0 2.9 %copy-start.20 = (f32[256,16]{0,1:T(8,128)S(1)}, f32[256,16]{0,1:T(8,128)}, u32[]{:S(2)}) copy-start(f32[256,16]{0,1:T(8,128)} %param.29) | copy-start | bytes 49156
  16.1 2.9 %copy-start.21 = (f32[256,16]{0,1:T(8,128)S(1)}, f32[256,16]{0,1:T(8,128)}, u32[]{:S(2)}) copy-start(f32[256,16]{0,1:T(8,128)} %param.30) | copy-start | bytes 49156
  16.1 4.4 %copy-start.24 = (f32[4,512]{1,0:T(4,128)S(1)}, f32[4,512]{1,0:T(4,128)}, u32[]{:S(2)}) copy-start(f32[4,512]{1,0:T(4,128)} %param.35) | copy-start | bytes 24580
  16.1 5.0 %copy-start.19 = (f32[4,1024]{1,0:T(4,128)S(1)}, f32[4,1024]{1,0:T(4,128)}, u32[]{:S(2)}) copy-start(f32[4,1024]{1,0:T(4,128)} %param.33) | copy-start | bytes 49156
  18.2 108.3 %all-gather.13.cloned.1.call-start = ((), (), s32[]{:S(2)}) async-start(), calls=%async_computation.4 | async-start | bytes 7864320 | tf_op jit(solution)/shard_map/all_gather | solution.py:180
  38.6 3.0 %copy-start.8 = (f32[2,128,4,128]{3,1,2,0:T(8,128)S(1)}, f32[2,128,4,128]{3,1,2,0:T(8,128)}, u32[]{:S(2)}) copy-start(f32[2,128,4,128]{3,1,2,0:T(8,128)} %copy.92) | copy-start | bytes 1572868
  41.8 3.1 %copy-start.28 = (f32[2,16]{1,0:T(2,128)S(1)}, f32[2,16]{1,0:T(2,128)}, u32[]{:S(2)}) copy-start(f32[2,16]{1,0:T(2,128)} %get-tuple-element.151) | copy-start | bytes 388
  44.9 5.9 %copy-start.29 = (f32[2]{0:T(128)S(1)}, f32[2]{0:T(128)}, u32[]{:S(2)}) copy-start(f32[2]{0:T(128)} %add_convert_fusion) | copy-start | bytes 28
  51.3 2.3 copy-start.32
  55.4 8.8 %copy-start.31 = (f32[16]{0:T(128)S(1)}, f32[16]{0:T(128)}, u32[]{:S(2)}) copy-start(f32[16]{0:T(128)} %get-tuple-element.84) | copy-start | bytes 196
  55.4 123.7 %all-gather.9.cloned.1.call-start = ((), (), s32[]{:S(2)}) async-start(), calls=%async_computation.2 | async-start | bytes 3932160 | tf_op jit(solution)/shard_map/all_gather | solution.py:209
  55.5 4.1 %collective-permute-start.1 = (bf16[16,64,128]{2,1,0:T(8,128)(2,1)S(1)}, bf16[16,64,128]{2,1,0:T(8,128)(2,1)S(1)}, u32[]{:S(2)}, u32[]{:S(2)}) collective-permute-start(bf16[16,64,128]{2,1,0:T(8,128)(2,1)S(1)} %convert_element_type.179), channel_id=1, source_target_pairs={{0,4},{4,8},{8,12},{12,16},{16,20},{20,24},{24,28},{1,5},{5,9},{9,... | collective-permute-start | bytes 786440 | tf_op jit(solution)/shard_map/ppermute | solution.py:18
  59.7 13.1 %collective-permute-start.3 = (bf16[16,64,128]{2,1,0:T(8,128)(2,1)S(1)}, bf16[16,64,128]{2,1,0:T(8,128)(2,1)S(1)}, u32[]{:S(2)}, u32[]{:S(2)}) collective-permute-start(bf16[16,64,128]{2,1,0:T(8,128)(2,1)S(1)} %collective-permute-done.1), channel_id=1, source_target_pairs={{0,4},{4,8},{8,12},{12,16},{16,20},{20,24},{24,28},{1,5},{5,9},{9,... | collective-permute-start | bytes 786440 | tf_op jit(solution)/shard_map/ppermute | solution.py:18
  64.2 5.2 %collective-permute-start.2 = (f32[16]{0:T(128)S(1)}, f32[16]{0:T(128)S(1)}, u32[]{:S(2)}, u32[]{:S(2)}) collective-permute-start(f32[16]{0:T(128)S(1)} %copy-done.31), channel_id=1, source_target_pairs={{0,4},{4,8},{8,12},{12,16},{16,20},{20,24},{24,28},{1,5},{5,9},{9,... | collective-permute-start | bytes 200 | tf_op jit(solution)/shard_map/ppermute | solution.py:18
  69.4 3.3 %collective-permute-start.4 = (f32[16]{0:T(128)S(1)}, f32[16]{0:T(128)S(1)}, u32[]{:S(2)}, u32[]{:S(2)}) collective-permute-start(f32[16]{0:T(128)S(1)} %collective-permute-done.2), channel_id=1, source_target_pairs={{0,4},{4,8},{8,12},{12,16},{16,20},{20,24},{24,28},{1,5},{5,9},{9,... | collective-permute-start | bytes 200 | tf_op jit(solution)/shard_map/ppermute | solution.py:18
  72.9 11.1 %collective-permute-start.5 = (bf16[16,64,128]{2,1,0:T(8,128)(2,1)S(1)}, bf16[16,64,128]{2,1,0:T(8,128)(2,1)S(1)}, u32[]{:S(2)}, u32[]{:S(2)}) collective-permute-start(bf16[16,64,128]{2,1,0:T(8,128)(2,1)S(1)} %fusion.72), channel_id=1, source_target_pairs={{0,8},{4,12},{8,16},{12,20},{16,24},{20,28},{1,9},{5,13},{9,17},{1... | collective-permute-start | bytes 786440 | tf_op jit(solution)/shard_map/ppermute | solution.py:18
  84.3 9.9 %collective-permute-start.7 = (bf16[16,64,128]{2,1,0:T(8,128)(2,1)S(1)}, bf16[16,64,128]{2,1,0:T(8,128)(2,1)S(1)}, u32[]{:S(2)}, u32[]{:S(2)}) collective-permute-start(bf16[16,64,128]{2,1,0:T(8,128)(2,1)S(1)} %fusion.74), channel_id=1, source_target_pairs={{0,16},{4,20},{8,24},{12,28},{1,17},{5,21},{9,25},{13,29},{2,18},{... | collective-permute-start | bytes 786440 | tf_op jit(solution)/shard_map/ppermute | solution.py:18
  89.7 4.5 %collective-permute-start.6 = (f32[16]{0:T(128)S(1)}, f32[16]{0:T(128)S(1)}, u32[]{:S(2)}, u32[]{:S(2)}) collective-permute-start(f32[16]{0:T(128)S(1)} %get-tuple-element.77), channel_id=1, source_target_pairs={{0,8},{4,12},{8,16},{12,20},{16,24},{20,28},{1,9},{5,13},{9,17},{1... | collective-permute-start | bytes 200 | tf_op jit(solution)/shard_map/ppermute | solution.py:18
  126.5 3.9 %copy-start.34 = (bf16[2,2048,256]{2,1,0:T(8,128)(2,1)S(1)}, bf16[2,2048,256]{2,1,0:T(8,128)(2,1)}, u32[]{:S(2)}) copy-start(bf16[2,2048,256]{2,1,0:T(8,128)(2,1)} %param.42) | copy-start | bytes 6291460
  130.4 1.8 copy-start.35
  132.3 3.0 %copy-start.30 = (f32[16]{0:T(128)S(1)}, f32[16]{0:T(128)}, u32[]{:S(2)}) copy-start(f32[16]{0:T(128)} %param.32) | copy-start | bytes 196
  135.2 5.9 %copy-start.4 = (bf16[256,2048]{1,0:T(8,128)(2,1)S(1)}, bf16[256,2048]{1,0:T(8,128)(2,1)}, u32[]{:S(2)}) copy-start(bf16[256,2048]{1,0:T(8,128)(2,1)} %copy-done.3) | copy-start | bytes 3145732
  135.2 85.1 %all-gather.7.cloned.1.call-start = ((), (), s32[]{:S(2)}) async-start(), calls=%async_computation.1 | async-start | bytes 3276800 | tf_op jit(solution)/shard_map/all_gather | solution.py:210
  140.5 2.5 %copy-start.36 = (bf16[2048,256]{1,0:T(8,128)(2,1)S(1)}, bf16[2048,256]{1,0:T(8,128)(2,1)}, u32[]{:S(2)}) copy-start(bf16[2048,256]{1,0:T(8,128)(2,1)} %param.46) | copy-start | bytes 3145732
  144.9 1.4 copy-start.11
  144.9 1.4 copy-start.13
  144.9 1.4 copy-start.27
  150.5 1.2 copy-start.6
  157.8 3.2 %copy-start.1 = (f32[256,1024]{0,1:T(8,128)S(1)}, f32[256,1024]{0,1:T(8,128)}, u32[]{:S(2)}) copy-start(f32[256,1024]{0,1:T(8,128)} %fusion.71) | copy-start | bytes 3145732
  157.8 3.2 %copy-start.16 = (f32[4,256]{1,0:T(4,128)S(1)}, f32[4,256]{1,0:T(4,128)}, u32[]{:S(2)}) copy-start(f32[4,256]{1,0:T(4,128)} %mul.377) | copy-start | bytes 12292
  160.9 2.0 copy-start.2
  160.9 2.0 copy-start.5
  161.0 2.0 copy-start.15
  161.0 2.0 copy-start.25
  184.4 4.7 %copy-start.14 = (f32[4,256]{1,0:T(4,128)S(1)}, f32[4,256]{1,0:T(4,128)}, u32[]{:S(2)}) copy-start(f32[4,256]{1,0:T(4,128)} %get-tuple-element.110) | copy-start | bytes 12292
  184.4 5.0 %copy-start.26 = (f32[256,4]{0,1:T(4,128)S(1)}, f32[256,4]{0,1:T(4,128)}, u32[]{:S(2)}) copy-start(f32[256,4]{0,1:T(4,128)} %param.41) | copy-start | bytes 12292
  184.4 5.0 %copy-start.18 = (s32[256,4]{0,1:T(4,128)S(1)}, s32[256,4]{0,1:T(4,128)}, u32[]{:S(2)}) copy-start(s32[256,4]{0,1:T(4,128)} %param.40) | copy-start | bytes 12292
  184.4 42.6 %all-to-all-start = ((bf16[8,192,512]{2,1,0:T(8,128)(2,1)}), bf16[8,192,512]{2,1,0:T(8,128)(2,1)}, u32[]{:S(2)}, u32[]{:S(2)}) async-start(bf16[8,192,512]{2,1,0:T(8,128)(2,1)} %pad_maximum_fusion.1), calls=%async_computation | async-start | bytes 3145728 | tf_op jit(solution)/shard_map/all_to_all | solution.py:225
  221.4 2.8 %copy-start.33 = (bf16[4096,512]{1,0:T(8,128)(2,1)S(1)}, bf16[4096,512]{1,0:T(8,128)(2,1)}, u32[]{:S(2)}) copy-start(bf16[4096,512]{1,0:T(8,128)(2,1)} %param.37) | copy-start | bytes 12582916
  229.5 2.6 %copy-start.10 = (bf16[1024,512]{1,0:T(8,128)(2,1)S(1)}, bf16[1024,512]{1,0:T(8,128)(2,1)}, u32[]{:S(2)}) copy-start(bf16[1024,512]{1,0:T(8,128)(2,1)} %param.47) | copy-start | bytes 3145732
  (3 other events, 3.4 us)
Sparse Core Ops, SparseCore 0:
  18.4 31.4 all-gather.10
  55.5 70.9 all-gather.12
  135.4 43.6 all-gather.8
  180.8 39.4 all-gather.6
